TPU v7x, 32 devices: a whole 2x2x4 slice. The times are simulated.
32 devices in a mesh: grp: 2 (over y), fs: 4 (over z), tp: 4 (over x, core).
Axes of the slice: x: 2, y: 2, z: 4, core: 2. Of those that a mesh axis runs over, the one named last changes fastest.
Arguments:
- tokens: bfloat16 [8192, 2048], P(('grp', 'fs', 'tp')), parts along dimension 0, may hold values from -6 to 6
- norm_gains: float32 [4, 2048], replicated, may hold values from 0.1 to 1.9
- query_weight: bfloat16 [2048, 2048], P('fs', 'tp'), may hold values from -0.125 to 0.125
- key_weight: bfloat16 [2048, 2048], P('fs', 'tp'), may hold values from -0.125 to 0.125
- value_weight: bfloat16 [2048, 4096], P('fs', 'tp'), may hold values from -0.125 to 0.125
- swish_weight: bfloat16 [2048, 4096], P('fs', 'tp'), may hold values from -0.125 to 0.125
- mixer_output: bfloat16 [4096, 2048], P('tp', 'fs'), may hold values from -0.09375 to 0.09375
- gate_weight: bfloat16 [2048, 3072], P('fs', 'tp'), may hold values from -0.125 to 0.125
- up_weight: bfloat16 [2048, 3072], P('fs', 'tp'), may hold values from -0.125 to 0.125
- down_weight: bfloat16 [3072, 2048], P('tp', 'fs'), may hold values from -0.109375 to 0.109375
Outputs:
- layer_output: bfloat16 [8192, 2048], P(('grp', 'fs', 'tp')), parts along dimension 0
There are 2 independent parts, one for each index of `grp`. A program takes and returns all parts, laid end to end along the dimension named above; an argument that names none is the same for every part. Nothing has to cross between parts.
All inputs are finite; a program needn't handle non-finite values.
Results may differ from a plain program's by a relative error of at most 0.02.
Values may be sent and summed in bfloat16 or wider, within the bound.
A program may use at most 128 MiB of HBM per device.

v0:
```python
import jax
import jax.numpy as jnp
from jax import lax
from jax.sharding import PartitionSpec as P

H = 8
QK = 256
BLOCK = 128
norm_epsilon = 1e-06
group_epsilon = 0.01


def rms_scale(matrix, gain):
    return (
        matrix * lax.rsqrt(jnp.mean(matrix * matrix, axis=-1, keepdims=True) + norm_epsilon) * gain
    )


def gather_rows(normed):
    return lax.all_gather(normed, "tp", axis=0, tiled=True)


def add_piece(normed, shard_piece):
    return jnp.dot(normed, shard_piece, preferred_element_type=jnp.float32)


def project_out(active, weight_shard):
    whole_weight = lax.all_gather(weight_shard, "fs", axis=1, tiled=True)
    return lax.psum_scatter(
        jnp.dot(active, whole_weight, preferred_element_type=jnp.float32).astype(jnp.bfloat16),
        "tp",
        scatter_dimension=0,
        tiled=True,
    ).astype(jnp.float32)


def rotate_halves(head_tensors, cosine_table, sine_table):
    half_width = head_tensors.shape[-1] // 2
    lower_half = head_tensors[..., :half_width]
    upper_half = head_tensors[..., half_width:]
    return jnp.concatenate(
        [
            lower_half * cosine_table - upper_half * sine_table,
            lower_half * sine_table + upper_half * cosine_table,
        ],
        axis=-1,
    )


def retention(queries, key_rows, value_rows, log_decay):
    length, head_count, key_width = queries.shape
    value_width = value_rows.shape[-1]
    blocks = length // BLOCK
    query_blocks = queries.reshape(blocks, BLOCK, head_count, key_width)
    key_blocks = key_rows.reshape(blocks, BLOCK, head_count, key_width)
    value_blocks = value_rows.reshape(blocks, BLOCK, head_count, value_width)
    offsets = jnp.arange(BLOCK, dtype=jnp.float32)
    distance = offsets[:, None] - offsets[None, :]
    within = jnp.where(
        distance >= 0, jnp.exp(log_decay[:, None, None] * jnp.maximum(distance, 0.0)), 0.0
    )
    retention_scores = jnp.einsum(
        "cnhd,cmhd->chnm", query_blocks, key_blocks, preferred_element_type=jnp.float32
    )
    local_part = jnp.einsum(
        "chnm,cmhe->cnhe", retention_scores * within[None], value_blocks.astype(jnp.float32)
    )
    key_decay = jnp.exp((BLOCK - 1.0 - offsets)[:, None] * log_decay[None, :])
    query_decay = jnp.exp((offsets + 1.0)[:, None] * log_decay[None, :])
    block_decay = jnp.exp(BLOCK * log_decay)

    def advance(carry_state, inputs):
        query_block, key_block, value_tile = inputs
        carried = (
            jnp.einsum("nhd,hde->nhe", query_block.astype(jnp.float32), carry_state)
            * query_decay[:, :, None]
        )
        decay_weighted = key_block.astype(jnp.float32) * key_decay[:, :, None]
        carry_state = carry_state * block_decay[:, None, None] + jnp.einsum(
            "yui,yua->uia", decay_weighted, value_tile.astype(jnp.float32)
        )
        return (carry_state, carried)

    starting_state = jnp.zeros((head_count, key_width, value_width), jnp.float32)
    _, carried = lax.scan(advance, starting_state, (query_blocks, key_blocks, value_blocks))
    return (local_part + carried).reshape(length, head_count, value_width)


def per_device(
    tokens,
    norm_gains,
    query_weight,
    key_weight,
    value_weight,
    swish_weight,
    mixer_output,
    gate_weight,
    up_weight,
    down_weight,
):
    residual = tokens.astype(jnp.float32)
    normed = gather_rows(rms_scale(residual, norm_gains[0]).astype(jnp.bfloat16))
    pieces = (
        lax.all_gather(query_weight, "fs", axis=0, tiled=True),
        lax.all_gather(key_weight, "fs", axis=0, tiled=True),
        lax.all_gather(value_weight, "fs", axis=0, tiled=True),
        lax.all_gather(swish_weight, "fs", axis=0, tiled=True),
    )
    raw_query, raw_keys, raw_values, raw_swish = tuple(
        (add_piece(normed, shard_piece) for shard_piece in pieces)
    )
    length = normed.shape[0]
    head_count = raw_query.shape[1] // QK
    positions = jnp.arange(length, dtype=jnp.float32)
    frequency = 10000.0 ** (-jnp.linspace(0.0, 1.0, QK // 2, dtype=jnp.float32))
    angles = positions[:, None] * frequency[None, :]
    cosine_table = jnp.cos(angles)[:, None, :]
    sine_table = jnp.sin(angles)[:, None, :]
    queries = rotate_halves(
        raw_query.reshape(length, head_count, QK), cosine_table, sine_table
    ).astype(jnp.bfloat16)
    key_rows = (
        rotate_halves(raw_keys.reshape(length, head_count, QK), cosine_table, sine_table)
        * QK ** (-0.5)
    ).astype(jnp.bfloat16)
    value_rows = raw_values.reshape(length, head_count, -1).astype(jnp.bfloat16)
    head_index = (lax.axis_index("tp") * head_count + jnp.arange(head_count)).astype(jnp.float32)
    log_decay = -(4.0 / BLOCK) * (BLOCK / (32.0 * length)) ** (head_index / (H - 1))
    retained = retention(queries, key_rows, value_rows, log_decay)
    centred = retained - jnp.mean(retained, axis=-1, keepdims=True)
    normalized = centred * lax.rsqrt(
        jnp.mean(centred * centred, axis=-1, keepdims=True) + group_epsilon
    )
    gated_rows = (jax.nn.silu(raw_swish) * normalized.reshape(length, -1)).astype(jnp.bfloat16)
    mixer_total = project_out(gated_rows, mixer_output)
    after_mixer = residual + rms_scale(mixer_total, norm_gains[1])
    widened = gather_rows(rms_scale(after_mixer, norm_gains[2]).astype(jnp.bfloat16))
    pieces = (
        lax.all_gather(gate_weight, "fs", axis=0, tiled=True),
        lax.all_gather(up_weight, "fs", axis=0, tiled=True),
    )
    gate_sum = add_piece(widened, pieces[0])
    up_sum = add_piece(widened, pieces[1])
    hidden = (jax.nn.silu(gate_sum) * up_sum).astype(jnp.bfloat16)
    channel = project_out(hidden, down_weight)
    return (after_mixer + rms_scale(channel, norm_gains[3])).astype(jnp.bfloat16)


def solution(mesh):
    placed = (
        P(("grp", "fs", "tp"), None),
        P(),
        P("fs", "tp"),
        P("fs", "tp"),
        P("fs", "tp"),
        P("fs", "tp"),
        P("tp", "fs"),
        P("fs", "tp"),
        P("fs", "tp"),
        P("tp", "fs"),
    )
    return jax.shard_map(
        per_device,
        mesh=mesh,
        in_specs=placed,
        out_specs=P(("grp", "fs", "tp"), None),
        check_vma=False,
    )
```

profile of v0, /device:TPU:0, one launch (start us, length us, event | category | flops | bytes accessed | tf_op | source)
XLA Modules:
  0.0 738.8 jit_solution(8517248313428038904)
XLA Ops:
  7.3 1.5 fusion.23
  9.8 2.5 fusion.25
  15.0 2.8 fusion.31
  18.0 39.4 %all-gather.17.cloned.1.call-done = bf16[2048,512]{1,0:T(8,128)(2,1)} async-done(((bf16[512,512]{1,0:T(8,128)(2,1)}), bf16[2048,512]{1,0:T(8,128)(2,1)}) %all-gather.17.cloned.1.call-update) | async-done | bytes 2097168 | tf_op jit(solution)/shard_map/all_gather | solution.py:104
  57.3 34.8 %all-gather.11.cloned.1.call-done = bf16[1024,2048]{1,0:T(8,128)(2,1)} async-done(((bf16[256,2048]{1,0:T(8,128)(2,1)}), bf16[1024,2048]{1,0:T(8,128)(2,1)}) %all-gather.11.cloned.1.call-update) | async-done | bytes 4194320 | tf_op jit(solution)/shard_map/all_gather | solution.py:20
  92.2 5.2 fusion.48
  97.6 1.3 copy.49
  98.9 1.3 copy.50
  100.2 39.2 %all-gather.19.cloned.1.call-done = bf16[2048,512]{1,0:T(8,128)(2,1)} async-done(((bf16[512,512]{1,0:T(8,128)(2,1)}), bf16[2048,512]{1,0:T(8,128)(2,1)}) %all-gather.19.cloned.1.call-update) | async-done | bytes 2097168 | tf_op jit(solution)/shard_map/all_gather | solution.py:105
  139.4 5.2 fusion.49
  144.8 1.3 copy.51
  146.1 1.3 copy.52
  147.5 4.4 subtract_convert_fusion
  154.0 66.5 %all-gather.15.cloned.1.call-done = bf16[2048,1024]{1,0:T(8,128)(2,1)} async-done(((bf16[512,1024]{1,0:T(8,128)(2,1)}), bf16[2048,1024]{1,0:T(8,128)(2,1)}) %all-gather.15.cloned.1.call-update) | async-done | bytes 4194320 | tf_op jit(solution)/shard_map/all_gather | solution.py:106
  220.4 9.3 %convolution_convert_fusion.2 = bf16[1024,1024]{1,0:T(8,128)(2,1)} fusion(bf16[1024,2048]{1,0:T(8,128)(2,1)} %all-gather.11.cloned.1.call-done, bf16[2048,1024]{1,0:T(8,128)(2,1)} %all-gather.15.cloned.1.call-done), kind=kOutput, calls=%fused_computation.53 | convolution fusion | flops 4296015872 | bytes 10485760 | tf_op jit(solution)/shard_map/dot_general | solution.py:24
  229.8 4.5 convert_element_type.66
  234.3 1.4 fusion.26
  235.8 31.7 %while.15 = (s32[]{:T(128)}, f32[2,256,512]{2,1,0:T(8,128)S(1)}, f32[8,128,2,512]{1,3,2,0:T(8,128)}, bf16[8,128,2,256]{3,1,2,0:T(8,128)(2,1)S(1)}, bf16[8,128,2,...) while((s32[]{:T(128)}, f32[2,256,512]{2,1,0:T(8,128)S(1)}, ...), condition=%wide.region_2.3_spmd.clone.clone.clone, body=%wide.region_1.2_spmd.clone.clone.clone.sunk | while | flops 135528960 | bytes 7346340 | solution.py:85
  235.8 1.1 fusion.71
  239.8 1.1 fusion.71
  241.0 1.1 constant_dynamic-slice_fusion.4
  247.8 1.1 fusion.71
  251.7 1.1 fusion.71
  263.6 1.1 fusion.71
  267.5 6.3 fusion.43
  273.8 7.2 copy.40
  281.0 2.6 multiply_reduce_fusion
  283.9 1.4 mul.345
  285.3 3.0 copy.61
  288.5 1.4 sub.74
  289.9 3.1 copy.60
  292.9 3.0 copy.59
  295.9 5.2 all-gather.13.cloned.1.call-done
  301.1 80.7 %all-gather.21.cloned.1.call-done = bf16[1024,2048]{1,0:T(8,128)(2,1)} async-done(((bf16[1024,512]{1,0:T(8,128)(2,1)}), bf16[1024,2048]{1,0:T(8,128)(2,1)}) %all-gather.21.cloned.1.call-update) | async-done | bytes 4194320 | tf_op jit(solution)/shard_map/all_gather | solution.py:28
  381.8 17.5 %convolution_convert_fusion.1 = bf16[1024,2048]{1,0:T(8,128)(2,1)} fusion(bf16[1024,2048]{1,0:T(8,128)(2,1)} %all-gather.21.cloned.1.call-done, f32[1024,1024]{1,0:T(8,128)} %bitcast.75, f32[1024,1024]{1,0:T(8,128)} %bitcast.77, f32[1024,1024]{1,0:T(8,128)} %bitcast.76, bf16[1024,2048]{1,0:T(8,128)(2,1)} %all-gather.11.cloned.1.call-done, ...), kind=kOutput, calls=%fused_computation.28 | convolution fusion | flops 8600420352 | bytes 29360128 | tf_op jit(solution)/shard_map/dot_general | solution.py:30
  400.1 42.4 %reduce-scatter.3.cloned.1.call-done = bf16[256,2048]{1,0:T(8,128)(2,1)} async-done(((bf16[1024,2048]{1,0:T(8,128)(2,1)}), bf16[256,2048]{1,0:T(8,128)(2,1)}) %reduce-scatter.3.cloned.1.call-update) | async-done | bytes 1048592 | tf_op jit(solution)/shard_map/reduce_scatter | solution.py:29
  442.6 1.6 fusion.17
  444.2 1.8 multiply_reduce_fusion.1
  446.0 1.6 multiply_convert_fusion.3
  449.2 58.4 %all-gather.25.cloned.1.call-done = bf16[2048,768]{1,0:T(8,128)(2,1)} async-done(((bf16[512,768]{1,0:T(8,128)(2,1)}), bf16[2048,768]{1,0:T(8,128)(2,1)}) %all-gather.25.cloned.1.call-update) | async-done | bytes 3145744 | tf_op jit(solution)/shard_map/all_gather | solution.py:139
  507.6 34.7 %all-gather.23.cloned.1.call-done = bf16[1024,2048]{1,0:T(8,128)(2,1)} async-done(((bf16[256,2048]{1,0:T(8,128)(2,1)}), bf16[1024,2048]{1,0:T(8,128)(2,1)}) %all-gather.23.cloned.1.call-update) | async-done | bytes 4194320 | tf_op jit(solution)/shard_map/all_gather | solution.py:20
  542.3 8.2 %fusion.50 = f32[1024,768]{1,0:T(8,128)} fusion(bf16[1024,2048]{1,0:T(8,128)(2,1)} %all-gather.23.cloned.1.call-done, bf16[2048,768]{1,0:T(8,128)(2,1)} %all-gather.25.cloned.1.call-done), kind=kOutput, calls=%fused_computation.91 | convolution fusion | flops 3221225472 | bytes 10485760 | tf_op jit(solution)/shard_map/dot_general | solution.py:24
  550.5 56.7 %all-gather.27.cloned.1.call-done = bf16[2048,768]{1,0:T(8,128)(2,1)} async-done(((bf16[512,768]{1,0:T(8,128)(2,1)}), bf16[2048,768]{1,0:T(8,128)(2,1)}) %all-gather.27.cloned.1.call-update) | async-done | bytes 3145744 | tf_op jit(solution)/shard_map/all_gather | solution.py:140
  607.2 63.7 %all-gather.29.cloned.1.call-done = bf16[768,2048]{1,0:T(8,128)(2,1)} async-done(((bf16[768,512]{1,0:T(8,128)(2,1)}), bf16[768,2048]{1,0:T(8,128)(2,1)}) %all-gather.29.cloned.1.call-update) | async-done | bytes 3145744 | tf_op jit(solution)/shard_map/all_gather | solution.py:28
  670.9 13.2 %convolution_convert_fusion = bf16[1024,2048]{1,0:T(8,128)(2,1)} fusion(bf16[768,2048]{1,0:T(8,128)(2,1)} %all-gather.29.cloned.1.call-done, f32[1024,768]{1,0:T(8,128)} %fusion.50, bf16[1024,2048]{1,0:T(8,128)(2,1)} %all-gather.23.cloned.1.call-done, bf16[2048,768]{1,0:T(8,128)(2,1)} %all-gather.27.cloned.1.call-done), kind=kOutput, calls=%fused_computation.27 | convolution fusion | flops 6449266688 | bytes 17825792 | tf_op jit(solution)/shard_map/dot_general | solution.py:30
  684.1 43.4 %reduce-scatter.5.cloned.1.call-done = bf16[256,2048]{1,0:T(8,128)(2,1)} async-done(((bf16[1024,2048]{1,0:T(8,128)(2,1)}), bf16[256,2048]{1,0:T(8,128)(2,1)}) %reduce-scatter.5.cloned.1.call-update) | async-done | bytes 1048592 | tf_op jit(solution)/shard_map/reduce_scatter | solution.py:29
  727.5 1.5 fusion.19
  729.0 2.9 fusion.22
  (122 shorter events, 34.2 us)
Async XLA Ops:
  6.5 50.8 %all-gather.17.cloned.1.call-start = ((), (), s32[]{:S(2)}) async-start(), calls=%async_computation.5 | async-start | bytes 2621440 | tf_op jit(solution)/shard_map/all_gather | solution.py:104
  7.3 84.9 %all-gather.11.cloned.1.call-start = ((), (), s32[]{:S(2)}) async-start(), calls=%async_computation.2 | async-start | bytes 5242880 | tf_op jit(solution)/shard_map/all_gather | solution.py:20
  12.3 127.1 %all-gather.19.cloned.1.call-start = ((), (), s32[]{:S(2)}) async-start(), calls=%async_computation.6 | async-start | bytes 2621440 | tf_op jit(solution)/shard_map/all_gather | solution.py:105
  13.0 207.4 %all-gather.15.cloned.1.call-start = ((), (), s32[]{:S(2)}) async-start(), calls=%async_computation.4 | async-start | bytes 5242880 | tf_op jit(solution)/shard_map/all_gather | solution.py:106
  13.6 287.5 %all-gather.13.cloned.1.call-start = ((), (), s32[]{:S(2)}) async-start(), calls=%async_computation.3 | async-start | bytes 5242880 | tf_op jit(solution)/shard_map/all_gather | solution.py:107
  14.2 367.6 %all-gather.21.cloned.1.call-start = ((), (), s32[]{:S(2)}) async-start(), calls=%async_computation.7 | async-start | bytes 5242880 | tf_op jit(solution)/shard_map/all_gather | solution.py:28
  14.8 427.8 %reduce-scatter.3.cloned.1.call-start = ((), (), s32[]{:S(2)}) async-start(), calls=%async_computation.8 | async-start | bytes 5242880 | tf_op jit(solution)/shard_map/reduce_scatter | solution.py:29
  151.8 0.8 copy-start.3
  151.8 1.0 copy-start.4
  289.9 3.1 copy-start.1
  399.3 44.9 %copy-start = (bf16[256,2048]{1,0:T(8,128)(2,1)S(1)}, bf16[256,2048]{1,0:T(8,128)(2,1)}, u32[]{:S(2)}) copy-start(bf16[256,2048]{1,0:T(8,128)(2,1)} %param.12) | copy-start | bytes 3145732
  399.3 108.3 %all-gather.25.cloned.1.call-start = ((), (), s32[]{:S(2)}) async-start(), calls=%async_computation.10 | async-start | bytes 3932160 | tf_op jit(solution)/shard_map/all_gather | solution.py:139
  400.1 142.2 %all-gather.23.cloned.1.call-start = ((), (), s32[]{:S(2)}) async-start(), calls=%async_computation.9 | async-start | bytes 5242880 | tf_op jit(solution)/shard_map/all_gather | solution.py:20
  442.5 3.5 copy-start.2
  447.6 159.5 %all-gather.27.cloned.1.call-start = ((), (), s32[]{:S(2)}) async-start(), calls=%async_computation.11 | async-start | bytes 3932160 | tf_op jit(solution)/shard_map/all_gather | solution.py:140
  448.2 222.7 %all-gather.29.cloned.1.call-start = ((), (), s32[]{:S(2)}) async-start(), calls=%async_computation.12 | async-start | bytes 3932160 | tf_op jit(solution)/shard_map/all_gather | solution.py:28
  449.0 278.5 %reduce-scatter.5.cloned.1.call-start = ((), (), s32[]{:S(2)}) async-start(), calls=%async_computation.13 | async-start | bytes 5242880 | tf_op jit(solution)/shard_map/reduce_scatter | solution.py:29
Sparse Core Ops, SparseCore 0:
  8.9 48.3 all-gather.16
  58.9 33.2 all-gather.10
  93.8 45.6 all-gather.18
  140.9 79.5 all-gather.14
  221.9 79.2 all-gather.12
  302.5 79.2 all-gather.20
  399.4 43.0 reduce-scatter.2
  444.1 63.4 all-gather.24
  509.2 33.0 all-gather.22
  543.7 63.4 all-gather.26
  608.8 62.0 all-gather.28
  684.2 43.2 reduce-scatter.4
where the time goes:
time: 740 us; the launch traced here: 739 us
  waiting for transfers between devices  570 us (77%)
  matrix products  77.2 us (10%)
  local copies, waits for them, and re-layouts  51 us (7%)
  other arithmetic  25.9 us (4%)
  between operations  13.7 us (2%)
    all_gather x2, waiting for transfers between devices, project_out(): whole_weight = lax.all_gather(weight_shard, 'fs', axis=1, tiled=True)  144 us
    reduce_scatter x2, waiting for transfers between devices, project_out(): lax.psum_scatter(jnp.dot(active, whole_weight, preferred_element_type=jnp...  85.8 us
    all_gather x2, waiting for transfers between devices, gather_rows(): return lax.all_gather(normed, 'tp', axis=0, tiled=True)  69.5 us
    all_gather x1, waiting for transfers between devices, per_device(): lax.all_gather(value_weight, 'fs', axis=0, tiled=True)  66.5 us
    all_gather x1, waiting for transfers between devices, per_device(): lax.all_gather(gate_weight, 'fs', axis=0, tiled=True)  58.4 us
    all_gather x1, waiting for transfers between devices, per_device(): lax.all_gather(up_weight, 'fs', axis=0, tiled=True)  56.7 us
    all_gather x1, waiting for transfers between devices, per_device(): lax.all_gather(query_weight, 'fs', axis=0, tiled=True)  39.4 us
    all_gather x1, waiting for transfers between devices, per_device(): lax.all_gather(key_weight, 'fs', axis=0, tiled=True)  39.2 us
  transfers between devices with their start and end apart: 12, of which 12 were waited for; matrix products, arithmetic and copies ran while one was open for 16% of the time, Pallas kernels for 0%

commit v1 on v0

--- a/solution.py
+++ b/solution.py
@@ -25,7 +25,12 @@
 
 
 def project_out(active, weight_shard):
-    whole_weight = lax.all_gather(weight_shard, "fs", axis=1, tiled=True)
+    ring = [weight_shard]
+    for hop in range(3):
+        ring.append(lax.ppermute(ring[-1], "fs", [(dev, (dev + 1) % 4) for dev in range(4)]))
+    whole_weight = jnp.roll(
+        jnp.concatenate(ring[::-1], axis=1), (lax.axis_index("fs") + 1) * ring[0].shape[1], axis=1
+    )
     return lax.psum_scatter(
         jnp.dot(active, whole_weight, preferred_element_type=jnp.float32).astype(jnp.bfloat16),
         "tp",

time: 740 us -> 646 us (0.87)
  waiting for transfers between devices: 570 us -> 418 us
  starting transfers between devices: 0.65 us -> 34.2 us
  local copies, waits for them, and re-layouts: 51 us -> 73.3 us
    ppermute x0 -> x6, waiting for transfers between devices: none -> 183 us  [project_out(): lax.ppermute(ring[-1], 'fs', [(dev, (dev + 1) % 4) for dev in range(4)])]
    all_gather x2 -> x0, waiting for transfers between devices: 144 us -> none  [project_out(): whole_weight = lax.all_gather(weight_shard, 'fs', axis=1, tiled=True)]
    all_gather x2, waiting for transfers between devices: 69.5 us -> 7.48 us  [gather_rows(): return lax.all_gather(normed, 'tp', axis=0, tiled=True)]
    all_gather x1, waiting for transfers between devices: 58.4 us -> 0.01 us  [per_device(): lax.all_gather(gate_weight, 'fs', axis=0, tiled=True)]
    all_gather x1, waiting for transfers between devices: 39.4 us -> 0.01 us  [per_device(): lax.all_gather(query_weight, 'fs', axis=0, tiled=True)]
    ppermute x0 -> x6, starting transfers between devices: none -> 33.8 us  [project_out(): lax.ppermute(ring[-1], 'fs', [(dev, (dev + 1) % 4) for dev in range(4)])]
    all_gather x1, waiting for transfers between devices: 39.2 us -> 10.6 us  [per_device(): lax.all_gather(key_weight, 'fs', axis=0, tiled=True)]
    unnamed x17 -> x35, local copies, waits for them, and re-layouts: 15.1 us -> 35.2 us
  transfers between devices with their start and end apart: 12 -> 16, of which waited for: 12 -> 13; matrix products, arithmetic and copies ran while one was open for 16% -> 22% of each run, Pallas kernels for 0% -> 0%
where the time goes in v1:
time: 646 us; the launch traced here: 644 us
  waiting for transfers between devices  418 us (65%)
  matrix products  77.1 us (12%)
  local copies, waits for them, and re-layouts  73.3 us (11%)
  starting transfers between devices  34.2 us (5%)
  other arithmetic  27 us (4%)
  between operations  13.8 us (2%)
    ppermute x6, waiting for transfers between devices, project_out(): lax.ppermute(ring[-1], 'fs', [(dev, (dev + 1) % 4) for dev in range(4)])  183 us
    reduce_scatter x2, waiting for transfers between devices, project_out(): lax.psum_scatter(jnp.dot(active, whole_weight, preferred_element_type=jnp...  85.8 us
    all_gather x1, waiting for transfers between devices, per_device(): lax.all_gather(value_weight, 'fs', axis=0, tiled=True)  66.2 us
    all_gather x1, waiting for transfers between devices, per_device(): lax.all_gather(up_weight, 'fs', axis=0, tiled=True)  56.9 us
    unnamed x35, local copies, waits for them, and re-layouts  35.2 us
    ppermute x6, starting transfers between devices, project_out(): lax.ppermute(ring[-1], 'fs', [(dev, (dev + 1) % 4) for dev in range(4)])  33.8 us
    dot_general x2, matrix products, project_out(): jnp.dot(active, whole_weight, preferred_element_type=jnp.float32)  30.6 us
    dot_general x4, matrix products, add_piece(): return jnp.dot(normed, shard_piece, preferred_element_type=jnp.float32)  28 us
  transfers between devices with their start and end apart: 16, of which 13 were waited for; matrix products, arithmetic and copies ran while one was open for 22% of the time, Pallas kernels for 0%

profile of v1, /device:TPU:0, one launch (start us, length us, event | category | flops | bytes accessed | tf_op | source)
XLA Modules:
  0.0 644.3 jit_solution(6298005504714603084)
XLA Ops:
  7.3 1.5 fusion.29
  9.8 2.5 fusion.31
  13.7 3.1 collective-permute-start
  16.8 44.1 %collective-permute-done = bf16[1024,512]{1,0:T(8,128)(2,1)S(1)} collective-permute-done((bf16[1024,512]{1,0:T(8,128)(2,1)S(1)}, bf16[1024,512]{1,0:T(8,128)(2,1)S(1)}, u32[]{:S(2)}, u32[]{:S(2)}) %collective-permute-start) | collective-permute-done | bytes 1048608 | tf_op jit(solution)/shard_map/ppermute | solution.py:30
  60.9 13.6 %collective-permute-start.1 = (bf16[1024,512]{1,0:T(8,128)(2,1)S(1)}, bf16[1024,512]{1,0:T(8,128)(2,1)}, u32[]{:S(2)}, u32[]{:S(2)}) collective-permute-start(bf16[1024,512]{1,0:T(8,128)(2,1)S(1)} %collective-permute-done), channel_id=1, source_target_pairs={{0,4},{4,8},{8,12},{12,0},{1,5},{5,9},{9,13},{13,1},{2,6},{6,10},{... | collective-permute-start | bytes 3145736 | tf_op jit(solution)/shard_map/ppermute | solution.py:30
  74.6 25.3 %collective-permute-done.1 = bf16[1024,512]{1,0:T(8,128)(2,1)} collective-permute-done((bf16[1024,512]{1,0:T(8,128)(2,1)S(1)}, bf16[1024,512]{1,0:T(8,128)(2,1)}, u32[]{:S(2)}, u32[]{:S(2)}) %collective-permute-start.1) | collective-permute-done | bytes 1048608 | tf_op jit(solution)/shard_map/ppermute | solution.py:30
  100.1 2.8 fusion.37
  103.0 24.2 %collective-permute-done.2 = bf16[1024,512]{1,0:T(8,128)(2,1)} collective-permute-done((bf16[1024,512]{1,0:T(8,128)(2,1)}, bf16[1024,512]{1,0:T(8,128)(2,1)}, u32[]{:S(2)}, u32[]{:S(2)}) %collective-permute-start.2) | collective-permute-done | bytes 1048608 | tf_op jit(solution)/shard_map/ppermute | solution.py:30
  127.1 2.4 constant_dynamic-update-slice_fusion.8
  129.5 2.3 constant_dynamic-update-slice_fusion.7
  134.1 2.4 constant_dynamic-update-slice_fusion.4
  136.5 2.4 constant_dynamic-update-slice_fusion.3
  141.1 5.3 fusion.56
  146.5 1.4 copy.49
  149.2 10.6 %all-gather.17.cloned.1.call-done = bf16[2048,512]{1,0:T(8,128)(2,1)} async-done(((bf16[512,512]{1,0:T(8,128)(2,1)}), bf16[2048,512]{1,0:T(8,128)(2,1)}) %all-gather.17.cloned.1.call-update) | async-done | bytes 2097168 | tf_op jit(solution)/shard_map/all_gather | solution.py:110
  159.8 5.2 fusion.57
  167.9 4.4 subtract_convert_fusion
  174.3 66.2 %all-gather.13.cloned.1.call-done = bf16[2048,1024]{1,0:T(8,128)(2,1)} async-done(((bf16[512,1024]{1,0:T(8,128)(2,1)}), bf16[2048,1024]{1,0:T(8,128)(2,1)}) %all-gather.13.cloned.1.call-update) | async-done | bytes 4194320 | tf_op jit(solution)/shard_map/all_gather | solution.py:111
  240.5 9.3 %convolution_convert_fusion.1 = bf16[1024,1024]{1,0:T(8,128)(2,1)} fusion(bf16[1024,2048]{1,0:T(8,128)(2,1)} %all-gather.9.cloned.1.call-done, bf16[2048,1024]{1,0:T(8,128)(2,1)} %all-gather.13.cloned.1.call-done), kind=kOutput, calls=%fused_computation.56 | convolution fusion | flops 4296015872 | bytes 10485760 | tf_op jit(solution)/shard_map/dot_general | solution.py:24
  249.8 4.6 convert_element_type.66
  254.5 1.4 fusion.32
  255.9 31.8 %while.15 = (s32[]{:T(128)}, f32[2,256,512]{2,1,0:T(8,128)S(1)}, f32[8,128,2,512]{1,3,2,0:T(8,128)}, bf16[8,128,2,256]{3,1,2,0:T(8,128)(2,1)S(1)}, bf16[8,128,2,...) while((s32[]{:T(128)}, f32[2,256,512]{2,1,0:T(8,128)S(1)}, ...), condition=%wide.region_2.3_spmd.clone.clone.clone, body=%wide.region_1.2_spmd.clone.clone.clone.sunk | while | flops 135528960 | bytes 7346340 | solution.py:90
  287.7 6.4 fusion.51
  294.1 7.2 %copy.40 = f32[8,128,2,512]{3,2,1,0:T(2,128)} copy(f32[8,128,2,512]{1,3,2,0:T(8,128)} %get-tuple-element.223) | data formatting | bytes 8388608 | tf_op jit(solution)/shard_map/add | solution.py:91
  301.4 2.6 multiply_reduce_fusion
  304.3 1.4 mul.349
  305.7 3.0 copy.61
  308.9 1.4 sub.80
  310.3 3.0 copy.60
  313.3 3.0 copy.59
  316.3 4.9 all-gather.11.cloned.1.call-done
  321.2 17.5 %fusion.19 = bf16[1024,2048]{1,0:T(8,128)(2,1)} fusion(bf16[1024,4096]{1,0:T(8,128)(2,1)} %constant_dynamic-update-slice_fusion.1, s32[]{:T(128)S(6)} %select_n.29, f32[1024,1024]{1,0:T(8,128)} %bitcast.73, f32[1024,1024]{1,0:T(8,128)} %bitcast.75, f32[1024,1024]{1,0:T(8,128)} %bitcast.74, bf16[1024,2048]{1,0:T(8,128)(2,1)} %all-gather.9.cloned.1.call-done, ...), kind=kOutput, calls=%fused_computation.29 | convolution fusion | flops 8600420352 | bytes 29360132 | tf_op jit(solution)/shard_map/dot_general | solution.py:35
  339.5 42.4 %reduce-scatter.3.cloned.1.call-done = bf16[256,2048]{1,0:T(8,128)(2,1)} async-done(((bf16[1024,2048]{1,0:T(8,128)(2,1)}), bf16[256,2048]{1,0:T(8,128)(2,1)}) %reduce-scatter.3.cloned.1.call-update) | async-done | bytes 1048592 | tf_op jit(solution)/shard_map/reduce_scatter | solution.py:34
  381.9 1.5 fusion.23
  383.5 1.8 multiply_reduce_fusion.1
  385.3 2.8 multiply_convert_fusion.3
  388.9 1.8 collective-permute-start.3
  390.7 34.9 %collective-permute-done.3 = bf16[768,512]{1,0:T(8,128)(2,1)S(1)} collective-permute-done((bf16[768,512]{1,0:T(8,128)(2,1)S(1)}, bf16[768,512]{1,0:T(8,128)(2,1)S(1)}, u32[]{:S(2)}, u32[]{:S(2)}) %collective-permute-start.3) | collective-permute-done | bytes 786464 | tf_op jit(solution)/shard_map/ppermute | solution.py:30
  425.5 15.4 %collective-permute-start.4 = (bf16[768,512]{1,0:T(8,128)(2,1)S(1)}, bf16[768,512]{1,0:T(8,128)(2,1)S(1)}, u32[]{:S(2)}, u32[]{:S(2)}) collective-permute-start(bf16[768,512]{1,0:T(8,128)(2,1)S(1)} %collective-permute-done.3), channel_id=1, source_target_pairs={{0,4},{4,8},{8,12},{12,0},{1,5},{5,9},{9,13},{13,1},{2,6},{6,10},{... | collective-permute-start | bytes 2359304 | tf_op jit(solution)/shard_map/ppermute | solution.py:30
  441.0 36.7 %collective-permute-done.4 = bf16[768,512]{1,0:T(8,128)(2,1)S(1)} collective-permute-done((bf16[768,512]{1,0:T(8,128)(2,1)S(1)}, bf16[768,512]{1,0:T(8,128)(2,1)S(1)}, u32[]{:S(2)}, u32[]{:S(2)}) %collective-permute-start.4) | collective-permute-done | bytes 786464 | tf_op jit(solution)/shard_map/ppermute | solution.py:30
  477.6 18.0 %collective-permute-done.5 = bf16[768,512]{1,0:T(8,128)(2,1)S(1)} collective-permute-done((bf16[768,512]{1,0:T(8,128)(2,1)S(1)}, bf16[768,512]{1,0:T(8,128)(2,1)S(1)}, u32[]{:S(2)}, u32[]{:S(2)}) %collective-permute-start.5) | collective-permute-done | bytes 786464 | tf_op jit(solution)/shard_map/ppermute | solution.py:30
  503.9 7.5 %all-gather.19.cloned.1.call-done = bf16[1024,2048]{1,0:T(8,128)(2,1)} async-done(((bf16[256,2048]{1,0:T(8,128)(2,1)}), bf16[1024,2048]{1,0:T(8,128)(2,1)}) %all-gather.19.cloned.1.call-update) | async-done | bytes 4194320 | tf_op jit(solution)/shard_map/all_gather | solution.py:20
  511.4 8.2 %fusion.58 = f32[1024,768]{1,0:T(8,128)} fusion(bf16[1024,2048]{1,0:T(8,128)(2,1)} %all-gather.19.cloned.1.call-done, bf16[2048,768]{1,0:T(8,128)(2,1)} %all-gather.21.cloned.1.call-done), kind=kOutput, calls=%fused_computation.112 | convolution fusion | flops 3221225472 | bytes 10485760 | tf_op jit(solution)/shard_map/dot_general | solution.py:24
  519.6 56.9 %all-gather.23.cloned.1.call-done = bf16[2048,768]{1,0:T(8,128)(2,1)} async-done(((bf16[512,768]{1,0:T(8,128)(2,1)}), bf16[2048,768]{1,0:T(8,128)(2,1)}) %all-gather.23.cloned.1.call-update) | async-done | bytes 3145744 | tf_op jit(solution)/shard_map/all_gather | solution.py:145
  576.4 13.1 %convolution_convert_fusion = bf16[1024,2048]{1,0:T(8,128)(2,1)} fusion(bf16[768,4096]{1,0:T(8,128)(2,1)} %constant_dynamic-update-slice_fusion.9, s32[]{:T(128)S(6)} %select_n.29, f32[1024,768]{1,0:T(8,128)} %fusion.58, bf16[1024,2048]{1,0:T(8,128)(2,1)} %all-gather.19.cloned.1.call-done, bf16[2048,768]{1,0:T(8,128)(2,1)} %all-gather.23.cloned.1.call-done), kind=kOutput, calls=%fused_computation.30 | convolution fusion | flops 6449266688 | bytes 17825796 | tf_op jit(solution)/shard_map/dot_general | solution.py:35
  589.6 43.4 %reduce-scatter.5.cloned.1.call-done = bf16[256,2048]{1,0:T(8,128)(2,1)} async-done(((bf16[1024,2048]{1,0:T(8,128)(2,1)}), bf16[256,2048]{1,0:T(8,128)(2,1)}) %reduce-scatter.5.cloned.1.call-update) | async-done | bytes 1048592 | tf_op jit(solution)/shard_map/reduce_scatter | solution.py:34
  633.0 1.5 fusion.25
  634.5 2.9 fusion.28
  (148 shorter events, 55.8 us)
Async XLA Ops:
  6.5 7.1 %copy-start.5 = (bf16[1024,512]{1,0:T(8,128)(2,1)S(1)}, bf16[1024,512]{1,0:T(8,128)(2,1)}, u32[]{:S(2)}) copy-start(bf16[1024,512]{1,0:T(8,128)(2,1)} %param.18) | copy-start | bytes 3145732
  6.5 134.6 %all-gather.15.cloned.1.call-start = ((), (), s32[]{:S(2)}) async-start(), calls=%async_computation.5 | async-start | bytes 2621440 | tf_op jit(solution)/shard_map/all_gather | solution.py:109
  7.3 133.8 %all-gather.9.cloned.1.call-start = ((), (), s32[]{:S(2)}) async-start(), calls=%async_computation.2 | async-start | bytes 5242880 | tf_op jit(solution)/shard_map/all_gather | solution.py:20
  12.3 147.5 %all-gather.17.cloned.1.call-start = ((), (), s32[]{:S(2)}) async-start(), calls=%async_computation.6 | async-start | bytes 2621440 | tf_op jit(solution)/shard_map/all_gather | solution.py:110
  13.0 227.5 %all-gather.13.cloned.1.call-start = ((), (), s32[]{:S(2)}) async-start(), calls=%async_computation.4 | async-start | bytes 5242880 | tf_op jit(solution)/shard_map/all_gather | solution.py:111
  13.6 307.6 %all-gather.11.cloned.1.call-start = ((), (), s32[]{:S(2)}) async-start(), calls=%async_computation.3 | async-start | bytes 5242880 | tf_op jit(solution)/shard_map/all_gather | solution.py:112
  13.7 47.3 %collective-permute-start = (bf16[1024,512]{1,0:T(8,128)(2,1)S(1)}, bf16[1024,512]{1,0:T(8,128)(2,1)S(1)}, u32[]{:S(2)}, u32[]{:S(2)}) collective-permute-start(bf16[1024,512]{1,0:T(8,128)(2,1)S(1)} %copy-done.5), channel_id=1, source_target_pairs={{0,4},{4,8},{8,12},{12,0},{1,5},{5,9},{9,13},{13,1},{2,6},{6,10},{... | collective-permute-start | bytes 3145736 | tf_op jit(solution)/shard_map/ppermute | solution.py:30
  60.9 38.9 %collective-permute-start.1 = (bf16[1024,512]{1,0:T(8,128)(2,1)S(1)}, bf16[1024,512]{1,0:T(8,128)(2,1)}, u32[]{:S(2)}, u32[]{:S(2)}) collective-permute-start(bf16[1024,512]{1,0:T(8,128)(2,1)S(1)} %collective-permute-done), channel_id=1, source_target_pairs={{0,4},{4,8},{8,12},{12,0},{1,5},{5,9},{9,13},{13,1},{2,6},{6,10},{... | collective-permute-start | bytes 3145736 | tf_op jit(solution)/shard_map/ppermute | solution.py:30
  74.5 307.4 %reduce-scatter.3.cloned.1.call-start = ((), (), s32[]{:S(2)}) async-start(), calls=%async_computation.7 | async-start | bytes 5242880 | tf_op jit(solution)/shard_map/reduce_scatter | solution.py:34
  99.8 27.3 %collective-permute-start.2 = (bf16[1024,512]{1,0:T(8,128)(2,1)}, bf16[1024,512]{1,0:T(8,128)(2,1)}, u32[]{:S(2)}, u32[]{:S(2)}) collective-permute-start(bf16[1024,512]{1,0:T(8,128)(2,1)} %collective-permute-done.1), channel_id=1, source_target_pairs={{0,4},{4,8},{8,12},{12,0},{1,5},{5,9},{9,13},{13,1},{2,6},{6,10},{... | collective-permute-start | bytes 3145736 | tf_op jit(solution)/shard_map/ppermute | solution.py:30
  172.2 0.8 copy-start.3
  172.2 1.0 copy-start.4
  310.3 3.0 copy-start.1
  338.7 44.8 %copy-start = (bf16[256,2048]{1,0:T(8,128)(2,1)S(1)}, bf16[256,2048]{1,0:T(8,128)(2,1)}, u32[]{:S(2)}) copy-start(bf16[256,2048]{1,0:T(8,128)(2,1)} %param.12) | copy-start | bytes 3145732
  338.7 165.2 %all-gather.21.cloned.1.call-start = ((), (), s32[]{:S(2)}) async-start(), calls=%async_computation.9 | async-start | bytes 3932160 | tf_op jit(solution)/shard_map/all_gather | solution.py:144
  339.4 49.5 %copy-start.6 = (bf16[768,512]{1,0:T(8,128)(2,1)S(1)}, bf16[768,512]{1,0:T(8,128)(2,1)}, u32[]{:S(2)}) copy-start(bf16[768,512]{1,0:T(8,128)(2,1)} %param.21) | copy-start | bytes 2359300
  339.4 171.9 %all-gather.19.cloned.1.call-start = ((), (), s32[]{:S(2)}) async-start(), calls=%async_computation.8 | async-start | bytes 5242880 | tf_op jit(solution)/shard_map/all_gather | solution.py:20
  388.1 188.3 %all-gather.23.cloned.1.call-start = ((), (), s32[]{:S(2)}) async-start(), calls=%async_computation.10 | async-start | bytes 3932160 | tf_op jit(solution)/shard_map/all_gather | solution.py:145
  388.9 244.1 %reduce-scatter.5.cloned.1.call-start = ((), (), s32[]{:S(2)}) async-start(), calls=%async_computation.11 | async-start | bytes 5242880 | tf_op jit(solution)/shard_map/reduce_scatter | solution.py:34
  388.9 36.6 %collective-permute-start.3 = (bf16[768,512]{1,0:T(8,128)(2,1)S(1)}, bf16[768,512]{1,0:T(8,128)(2,1)S(1)}, u32[]{:S(2)}, u32[]{:S(2)}) collective-permute-start(bf16[768,512]{1,0:T(8,128)(2,1)S(1)} %copy-done.6), channel_id=1, source_target_pairs={{0,4},{4,8},{8,12},{12,0},{1,5},{5,9},{9,13},{13,1},{2,6},{6,10},{... | collective-permute-start | bytes 2359304 | tf_op jit(solution)/shard_map/ppermute | solution.py:30
  425.5 52.1 %collective-permute-start.4 = (bf16[768,512]{1,0:T(8,128)(2,1)S(1)}, bf16[768,512]{1,0:T(8,128)(2,1)S(1)}, u32[]{:S(2)}, u32[]{:S(2)}) collective-permute-start(bf16[768,512]{1,0:T(8,128)(2,1)S(1)} %collective-permute-done.3), channel_id=1, source_target_pairs={{0,4},{4,8},{8,12},{12,0},{1,5},{5,9},{9,13},{13,1},{2,6},{6,10},{... | collective-permute-start | bytes 2359304 | tf_op jit(solution)/shard_map/ppermute | solution.py:30
  477.6 18.0 %collective-permute-start.5 = (bf16[768,512]{1,0:T(8,128)(2,1)S(1)}, bf16[768,512]{1,0:T(8,128)(2,1)S(1)}, u32[]{:S(2)}, u32[]{:S(2)}) collective-permute-start(bf16[768,512]{1,0:T(8,128)(2,1)S(1)} %collective-permute-done.4), channel_id=1, source_target_pairs={{0,4},{4,8},{8,12},{12,0},{1,5},{5,9},{9,13},{13,1},{2,6},{6,10},{... | collective-permute-start | bytes 2359304 | tf_op jit(solution)/shard_map/ppermute | solution.py:30
  589.6 44.9 %copy-start.2 = (bf16[256,2048]{1,0:T(8,128)(2,1)S(1)}, bf16[256,2048]{1,0:T(8,128)(2,1)}, u32[]{:S(2)}) copy-start(bf16[256,2048]{1,0:T(8,128)(2,1)} %reduce-scatter.3.cloned.1.call-done) | copy-start | bytes 3145732
Sparse Core Ops, SparseCore 0:
  8.9 67.2 all-gather.14
  77.8 32.7 all-gather.8
  112.1 47.6 all-gather.16
  161.2 79.2 all-gather.12
  241.9 79.2 all-gather.10
  338.8 43.0 reduce-scatter.2
  383.5 94.5 all-gather.20
  479.6 31.7 all-gather.18
  513.0 63.4 all-gather.22
  589.7 43.2 reduce-scatter.4
